TPU v7x, 32 devices: a whole 2x2x4 slice. The times are simulated.
32 devices in a mesh: ep: 8 (over z, y), tp: 4 (over x, core).
Axes of the slice: x: 2, y: 2, z: 4, core: 2. Of those that a mesh axis runs over, the one named last changes fastest.
Arguments:
- tokens: bfloat16 [384, 2048], P('ep'), may hold values from -6 to 6
- out_grad: bfloat16 [384, 2048], P('ep'), may hold values from -4 to 4
- expert_ids: int32 [384, 4], P('ep'), may hold values from 0 to 7, all different within a row; in each aligned block of 48 rows (0 to 47, 48 to 95, ...) at most 48 rows name the same one
- router_weight: bfloat16 [2048, 8], replicated, may hold values from -0.125 to 0.125
- w_gate: bfloat16 [8, 2048, 1536], P('ep', None, 'tp'), may hold values from -0.125 to 0.125
- w_up: bfloat16 [8, 2048, 1536], P('ep', None, 'tp'), may hold values from -0.125 to 0.125
- w_down: bfloat16 [8, 1536, 2048], P('ep', 'tp'), may hold values from -0.15625 to 0.15625
Outputs:
- token_grad: bfloat16 [384, 2048], P('ep', 'tp')
- router_grad: float32 [2048, 8], P('tp', 'ep')
- w_gate_grad: bfloat16 [8, 2048, 1536], P('ep', None, 'tp')
- w_up_grad: bfloat16 [8, 2048, 1536], P('ep', None, 'tp')
- w_down_grad: bfloat16 [8, 1536, 2048], P('ep', 'tp')
Inputs may be any that keep to these rules, and one draw needn't show every extreme that they name: `expert_ids`: each row names 4 different experts; among the rows of one device no expert is named more than 48 times, and in some devices' rows one expert is named exactly 48 times.
All inputs are finite; a program needn't handle non-finite values.
Results may differ from a plain program's by a relative error of at most 0.0058.
Values may be sent and summed in bfloat16 or wider, within the bound.
A program may use at most 128 MiB of HBM per device.

v0:
```python
import functools
import jax
import jax.numpy as jnp
from jax import lax
from jax.experimental import pallas as pl
from jax.experimental.pallas import tpu as pltpu
from jax.sharding import PartitionSpec as P

MESH = pl.DeviceIdType.MESH


def activation_parts(gate_pre, up_pre):
    glu = jnp.minimum(gate_pre, 7.0)
    linear = jnp.clip(up_pre, -7.0, 7.0)
    sigma = jax.nn.sigmoid(1.702 * glu)
    act_value = glu * sigma
    hidden = (linear + 1.0) * act_value
    slope = (linear + 1.0) * (sigma + 1.702 * glu * sigma * (1.0 - sigma))
    slope = jnp.where(gate_pre < 7.0, slope, 0.0)
    up_slope = jnp.where((up_pre > -7.0) & (up_pre < 7.0), act_value, 0.0)
    return (hidden, slope, up_slope)


def contract_last(left, right):
    return lax.dot_general(
        left, right, (((1,), (1,)), ((), ())), preferred_element_type=jnp.float32
    )


def contract_first(left, right):
    return lax.dot_general(
        left, right, (((0,), (0,)), ((), ())), preferred_element_type=jnp.float32
    )


def slotted(tokens, out_grad, expert_ids, router_weight, w_gate, w_up, w_down):
    tok_dev, model_width = tokens.shape
    top_count = expert_ids.shape[1]
    expert_count = router_weight.shape[1]
    peer_count = lax.axis_size("ep")
    tp_count = lax.axis_size("tp")
    capacity = min(
        tok_dev,
        tp_count * max(1, (2 * tok_dev * top_count // expert_count + tp_count - 1) // tp_count),
    )
    feature_part = model_width // tp_count
    logits = jnp.dot(tokens, router_weight, preferred_element_type=jnp.float32)
    chosen = jnp.take_along_axis(logits, expert_ids, axis=1)
    gate_values = jax.nn.softmax(chosen, axis=-1)
    flat_ids = expert_ids.reshape(-1)
    one_hot = (flat_ids[:, None] == jnp.arange(expert_count, dtype=jnp.int32)[None, :]).astype(
        jnp.int32
    )
    slot_rank = jnp.sum((jnp.cumsum(one_hot, axis=0) - one_hot) * one_hot, axis=1)
    slot_index = flat_ids * capacity + slot_rank
    flat_tok = jnp.arange(tok_dev * top_count, dtype=jnp.int32) // top_count
    buffer_rows = expert_count * capacity
    sent_tokens = (
        jnp.zeros((buffer_rows, model_width), jnp.bfloat16).at[slot_index].set(tokens[flat_tok])
    )
    sent_grads = (
        jnp.zeros((buffer_rows, model_width), jnp.bfloat16).at[slot_index].set(out_grad[flat_tok])
    )
    sent_gates = jnp.zeros((buffer_rows,), jnp.float32).at[slot_index].set(gate_values.reshape(-1))
    slot_tokens = sent_tokens.reshape(expert_count, capacity, model_width)
    slot_grads = sent_grads.reshape(expert_count, capacity, model_width)
    slot_gates = sent_gates.reshape(expert_count, capacity)
    slot_share = capacity // tp_count
    share_start = lax.axis_index("tp") * slot_share
    part_tokens = lax.dynamic_slice_in_dim(slot_tokens, share_start, slot_share, 1)
    part_grads = lax.dynamic_slice_in_dim(slot_grads, share_start, slot_share, 1)
    part_gates = lax.dynamic_slice_in_dim(slot_gates, share_start, slot_share, 1)
    got_tokens, got_grads = (
        lax.all_to_all(part_tokens, "ep", split_axis=0, concat_axis=0, tiled=True),
        lax.all_to_all(part_grads, "ep", split_axis=0, concat_axis=0, tiled=True),
    )
    got_gates = lax.all_to_all(part_gates, "ep", split_axis=0, concat_axis=0, tiled=True)
    recv_tokens, recv_grads = (
        lax.all_gather(got_tokens, "tp", axis=1, tiled=True),
        lax.all_gather(got_grads, "tp", axis=1, tiled=True),
    )
    recv_gates = lax.all_gather(got_gates, "tp", axis=1, tiled=True)
    slot_count = peer_count * capacity
    inputs_rows = recv_tokens.reshape(slot_count, model_width)
    grad_rows = recv_grads.reshape(slot_count, model_width)
    weight_rows = recv_gates.reshape(slot_count)
    gate_mat = w_gate[0]
    up_mat = w_up[0]
    down_mat = w_down[0]
    gate_pre = jnp.dot(inputs_rows, gate_mat, preferred_element_type=jnp.float32)
    up_pre = jnp.dot(inputs_rows, up_mat, preferred_element_type=jnp.float32)
    hidden, slope, up_slope = activation_parts(gate_pre, up_pre)
    back_proj = contract_last(grad_rows, down_mat)
    gate_score = jnp.sum(hidden * back_proj, axis=1)
    d_hidden = weight_rows[:, None] * back_proj
    d_gate_pre = (d_hidden * slope).astype(jnp.bfloat16)
    d_up_pre = (d_hidden * up_slope).astype(jnp.bfloat16)
    weighted = (weight_rows[:, None] * hidden).astype(jnp.bfloat16)
    w_down_grad = contract_first(weighted, grad_rows).astype(jnp.bfloat16)[None]
    w_gate_grad = contract_first(inputs_rows, d_gate_pre).astype(jnp.bfloat16)[None]
    w_up_grad = contract_first(inputs_rows, d_up_pre).astype(jnp.bfloat16)[None]
    summed_part = lax.psum_scatter(
        contract_last(gate_mat, d_gate_pre) + contract_last(up_mat, d_up_pre),
        "tp",
        scatter_dimension=0,
        tiled=True,
    )
    returned = summed_part.T.reshape(peer_count, capacity, feature_part)
    home_grads, home_scores = (
        lax.all_to_all(returned, "ep", split_axis=0, concat_axis=0, tiled=True),
        lax.all_to_all(
            gate_score.reshape(peer_count, capacity), "ep", split_axis=0, concat_axis=0, tiled=True
        ),
    )
    picked = home_grads.reshape(buffer_rows, feature_part)[slot_index]
    expert_part = jnp.sum(picked.reshape(tok_dev, top_count, feature_part), axis=1)
    local_scores = home_scores.reshape(buffer_rows)[slot_index].reshape(tok_dev, top_count)
    total_scores = lax.psum(local_scores, "tp")
    d_chosen = gate_values * (
        total_scores - jnp.sum(gate_values * total_scores, axis=-1, keepdims=True)
    )
    expert_hot = (
        expert_ids[:, :, None] == jnp.arange(expert_count, dtype=jnp.int32)[None, None, :]
    ).astype(jnp.float32)
    d_logits = jnp.sum(d_chosen[:, :, None] * expert_hot, axis=1)
    column = lax.axis_index("tp") * feature_part
    local_tokens = lax.dynamic_slice_in_dim(tokens, column, feature_part, 1).astype(jnp.float32)
    router_term = jnp.dot(local_tokens.T, d_logits, precision=lax.Precision.HIGHEST)
    router_grad = lax.psum_scatter(router_term, "ep", scatter_dimension=1, tiled=True)
    router_rows = lax.dynamic_slice_in_dim(router_weight, column, feature_part, 0).astype(
        jnp.float32
    )
    router_part = jnp.dot(d_logits, router_rows.T, precision=lax.Precision.HIGHEST)
    token_grad = (expert_part + router_part).astype(jnp.bfloat16)
    return (token_grad, router_grad, w_gate_grad, w_up_grad, w_down_grad)


def dense_kernel(
    tok_ref, og_ref, ids_ref, rw_ref, wg_ref, wu_ref, wd_ref,
    tgrad_ref, rgrad_ref, wgg, wug, wdg,
    rows_v, wg, wu, wd, gates, dpre, weighted, part_scores, tp_scores, scores, dlog,
    own_part, mate_out, mate_in, x_out, x_in, y_out, y_in, z_out, z_in,
    load_sem, z_s, z_r, y_s, y_r, x_s, x_r, m_s, m_r,
    g_s, g_r, t_s, t_r, s_s, s_r, rm_s, rm_r, rx_s, rx_r, ry_s, ry_r, rz_s, rz_r,
):
    block, width = tok_ref.shape
    units = wd.shape[0]
    n_ep, experts, lanes = gates.shape
    n_tp = lax.axis_size("tp")
    n_z = n_ep // 2
    pair = 2 * block
    feat = width // n_tp
    ep = lax.axis_index("ep")
    tp = lax.axis_index("tp")
    z, y = ep // 2, ep % 2
    x, core = tp // 2, tp % 2
    y_dev = (z * 2 + 1 - y, tp)
    x_dev = (ep, (1 - x) * 2 + core)
    m_dev = (ep, x * 2 + 1 - core)

    def z_dev(hop):
        return (((z + hop) % n_z) * 2 + y, tp)

    def ep_dev(hop):
        return ((ep + hop) % n_ep, tp)

    def tp_dev(hop):
        return (ep, (tp + hop) % n_tp)

    def remote(src, dst, send, recv, dev):
        return pltpu.make_async_remote_copy(
            src_ref=src, dst_ref=dst, send_sem=send, recv_sem=recv,
            device_id=dev, device_id_type=MESH,
        )

    def cols(quarter):
        return pl.ds(pl.multiple_of(quarter * feat, feat), feat)

    def rows(start, count):
        return pl.ds(pl.multiple_of(start * block, block), count * block)

    mine = rows(ep, 1)
    loads = [
        pltpu.make_async_copy(tok_ref, rows_v.at[0, mine, :], load_sem.at[0]),
        pltpu.make_async_copy(og_ref, rows_v.at[1, mine, :], load_sem.at[1]),
        pltpu.make_async_copy(wg_ref.at[0], wg, load_sem.at[2]),
        pltpu.make_async_copy(wu_ref.at[0], wu, load_sem.at[3]),
        pltpu.make_async_copy(wd_ref.at[0], wd, load_sem.at[4]),
    ]
    for load in loads:
        load.start()
    barrier = pltpu.get_barrier_semaphore()
    partners = [ep_dev(k) for k in range(1, n_ep)] + [tp_dev(k) for k in range(1, n_tp)]
    for dev in partners:
        pl.semaphore_signal(barrier, inc=1, device_id=dev, device_id_type=MESH)
    pl.semaphore_wait(barrier, len(partners))
    sent = []

    def launch(copy):
        copy.start()
        sent.append(copy)

    loads[0].wait()
    loads[1].wait()
    own_q, other_q = cols(tp), cols((1 - x) * 2 + core)

    def piece(first, count, quarter):
        return rows_v.at[:, rows(first, count), quarter]

    def z_copy(hop, first):
        p = piece(first, 1, own_q)
        return remote(p, p, z_s.at[hop], z_r.at[hop], z_dev(hop))

    def y_copy(c, first):
        p = piece(first, 1, own_q)
        return remote(p, p, y_s.at[c], y_r.at[c], y_dev)

    def x_copy(c, which, first, quarter=None):
        p = piece(first, 1, own_q if quarter is None else quarter)
        return remote(p, p, x_s.at[c, which], x_r.at[c, which], x_dev)

    def m_copy(c, which, first, count, quarter):
        p = piece(first, count, quarter)
        return remote(p, p, m_s.at[c, which], m_r.at[c, which], m_dev)

    mate_q = (cols(x * 2 + 1 - core), cols((1 - x) * 2 + 1 - core))
    launch(y_copy(0, ep))
    order = [0] + sorted(range(1, n_z), key=lambda c: min(c, n_z - c))
    for c in order[1:]:
        launch(z_copy(c, ep))

    logits = contract_last(rw_ref[...], rows_v[0, mine, :])
    expert = lax.broadcasted_iota(jnp.int32, (experts, block), 0)
    hot = jnp.zeros((experts, block), jnp.float32)
    for k in range(ids_ref.shape[0]):
        hot = jnp.where(ids_ref[k : k + 1, :] == expert, 1.0, hot)
    top = jnp.max(jnp.where(hot > 0.0, logits, -jnp.inf), axis=0, keepdims=True)
    expd = jnp.where(hot > 0.0, jnp.exp(jnp.where(hot > 0.0, logits - top, 0.0)), 0.0)
    gate_rows = expd / jnp.sum(expd, axis=0, keepdims=True)
    gates[ep] = jnp.zeros((experts, lanes), jnp.float32)
    gates[ep, :, 0:block] = gate_rows

    def gate_copy(hop, src):
        return remote(gates.at[src], gates.at[src], g_s.at[hop], g_r.at[hop], ep_dev(hop))

    for hop in range(1, n_ep):
        launch(gate_copy(hop, ep))

    for c in order:
        zs = (z + n_z - c) % n_z
        a, b = zs * 2 + y, zs * 2 + 1 - y
        if c > 0:
            z_copy(c, a).wait_recv()
            launch(y_copy(c, a))
            launch(x_copy(c, 0, a))
        y_copy(c, b).wait_recv()
        launch(x_copy(c, 1, b))
        if c > 0:
            launch(m_copy(c, 0, zs * 2, 2, own_q))
        else:
            launch(m_copy(c, 0, b, 1, own_q))
    for hop in range(1, n_ep):
        gate_copy(hop, (ep + n_ep - hop) % n_ep).wait_recv()
    for load in loads[2:]:
        load.wait()

    def tp_score_copy(hop):
        return remote(part_scores, tp_scores.at[hop], t_s.at[hop], t_r.at[hop], tp_dev(hop))

    def score_copy(hop, src):
        return remote(scores.at[src], scores.at[src], s_s.at[hop], s_r.at[hop], ep_dev(hop))

    def back_mate(c):
        return remote(mate_out.at[c], mate_in.at[c], rm_s.at[c], rm_r.at[c], m_dev)

    def crossed(c):
        return order.index(c) % 2 == 1

    def back_x(c):
        return remote(x_out.at[c], x_in.at[c], rx_s.at[c], rx_r.at[c], y_dev if crossed(c) else x_dev)

    def back_y(c):
        return remote(y_out.at[c], y_in.at[c], ry_s.at[c], ry_r.at[c], x_dev if crossed(c) else y_dev)

    def back_z(c):
        return remote(z_out.at[c], z_in.at[c], rz_s.at[c], rz_r.at[c], z_dev(n_z - c))

    def produce(c):
        here = rows((z + n_z - c) % n_z * 2, 2)
        dg = dpre[here, 0:units]
        du = dpre[here, units : 2 * units]
        for half in range(2):
            for side in range(2):
                q = half * 2 + (1 - core if side == 0 else core)
                span = cols(q)
                value = contract_last(dg, wg[span, :]) + contract_last(du, wu[span, :])
                if side == 0:
                    mate_out[c, half] = value.astype(jnp.bfloat16)
                else:
                    own_part[c, half] = value
        launch(back_mate(c))

    def after_mate(c):
        back_mate(c).wait_recv()
        if crossed(c):
            theirs = rows(1 - y, 1)
            for half in range(2):
                x_out[c, half * block : (half + 1) * block] = (
                    own_part[c, half, theirs, :] + mate_in[c, half, theirs, :].astype(jnp.float32)
                ).astype(jnp.bfloat16)
        else:
            x_out[c] = (own_part[c, 1 - x] + mate_in[c, 1 - x].astype(jnp.float32)).astype(jnp.bfloat16)
        launch(back_x(c))

    def after_x(c):
        back_x(c).wait_recv()
        if crossed(c):
            for half in range(2):
                own_part[c, half, rows(y, 1), :] = (
                    own_part[c, half, rows(y, 1), :]
                    + mate_in[c, half, rows(y, 1), :].astype(jnp.float32)
                    + x_in[c, half * block : (half + 1) * block].astype(jnp.float32)
                )
            y_out[c] = own_part[c, 1 - x, rows(y, 1), :].astype(jnp.bfloat16)
        else:
            total = own_part[c, x] + mate_in[c, x].astype(jnp.float32) + x_in[c].astype(jnp.float32)
            own_part[c, x] = total
            y_out[c] = own_part[c, x, rows(1 - y, 1), :].astype(jnp.bfloat16)
        launch(back_y(c))

    home = {}

    def after_y(c):
        back_y(c).wait_recv()
        total = own_part[c, x, rows(y, 1), :] + y_in[c].astype(jnp.float32)
        if c > 0:
            z_out[c] = total.astype(jnp.bfloat16)
            launch(back_z(c))
        else:
            home[0] = total

    tiles = 8
    tile = width // tiles

    def in_grad(i):
        span = pl.ds(i * tile, tile)
        value = contract_first(rows_v[0, :, span], dpre[...]).astype(jnp.bfloat16)
        wgg[0, span, :] = value[:, 0:units]
        wug[0, span, :] = value[:, units : 2 * units]

    def down_grad(i):
        span = pl.ds(i * feat, feat)
        wdg[0, :, span] = contract_first(weighted[...], rows_v[1, :, span]).astype(jnp.bfloat16)

    for c in order:
        zs = (z + n_z - c) % n_z
        a, b = zs * 2 + y, zs * 2 + 1 - y
        first, count = (zs * 2, 2) if c > 0 else (b, 1)
        if c > 0:
            x_copy(c, 0, a, other_q).wait_recv()
        x_copy(c, 1, b, other_q).wait_recv()
        launch(m_copy(c, 1, first, count, other_q))
        if c != order[0]:
            produce(previous)
        m_copy(c, 0, first, count, mate_q[0]).wait_recv()
        m_copy(c, 1, first, count, mate_q[1]).wait_recv()
        here = rows(zs * 2, 2)
        in_rows = rows_v[0, here, :]
        grad_rows = rows_v[1, here, :]
        gate_pre = jnp.dot(in_rows, wg[...], preferred_element_type=jnp.float32)
        up_pre = jnp.dot(in_rows, wu[...], preferred_element_type=jnp.float32)
        back = contract_last(grad_rows, wd[...])
        hidden, slope, up_slope = activation_parts(gate_pre, up_pre)
        columns = []
        for i in range(2):
            row = gates[zs * 2 + i, pl.ds(ep, 1), :]
            columns.append(jnp.broadcast_to(row, (lanes, lanes)).T[:block])
        weight = jnp.concatenate(columns, axis=0)
        weight = jnp.concatenate([weight] * (units // lanes), axis=1)
        product = hidden * back
        folded = product[:, 0:lanes]
        for i in range(1, units // lanes):
            folded = folded + product[:, i * lanes : (i + 1) * lanes]
        for i in range(2):
            tall = jnp.concatenate(
                [folded[i * block : (i + 1) * block], jnp.zeros((lanes - block, lanes), jnp.float32)],
                axis=0,
            )
            part_scores[pl.ds(zs * 2 + i, 1), :] = jnp.sum(tall.T, axis=0, keepdims=True)
        d_hidden = weight * back
        dpre[here, 0:units] = (d_hidden * slope).astype(jnp.bfloat16)
        dpre[here, units : 2 * units] = (d_hidden * up_slope).astype(jnp.bfloat16)
        weighted[here, :] = (weight * hidden).astype(jnp.bfloat16)
        if c != order[0]:
            after_mate(previous)
        previous = c

    for hop in range(1, n_tp):
        launch(tp_score_copy(hop))
    pieces = [functools.partial(in_grad, i) for i in range(tiles)]
    pieces += [functools.partial(down_grad, i) for i in range(n_tp)]

    def work(amount):
        for piece in pieces[:amount]:
            piece()
        del pieces[:amount]

    produce(order[-1])
    work(2)
    after_mate(order[-1])
    total = part_scores[...]
    for hop in range(1, n_tp):
        tp_score_copy(hop).wait_recv()
        total = total + tp_scores[hop]
    scores[ep] = total
    for hop in range(1, n_ep):
        launch(score_copy(hop, ep))
    work(2)
    for i, c in enumerate(order):
        after_x(c)
        if i > 0:
            after_y(order[i - 1])
        if i < n_z - 1:
            work(3)
    work(len(pieces))
    for hop in range(1, n_ep):
        score_copy(hop, (ep + n_ep - hop) % n_ep).wait_recv()
    score = scores[...]
    my_row = lax.broadcasted_iota(jnp.int32, (experts, lanes), 0) == ep
    router = jnp.zeros((experts, feat), jnp.float32)
    for s in range(n_ep):
        gate = gates[s]
        here = score[:, s, :]
        d_log = gate * (here - jnp.sum(gate * here, axis=0, keepdims=True))
        dlog[s] = d_log
        router = router + jnp.dot(
            jnp.where(my_row, d_log, 0.0)[:, 0:block],
            rows_v[0, s * block : (s + 1) * block, own_q].astype(jnp.float32),
            precision=lax.Precision.HIGHEST,
            preferred_element_type=jnp.float32,
        )
    rgrad_ref[...] = jnp.sum(router, axis=0, keepdims=True)
    term = jnp.dot(
        dlog[ep].T[0:block],
        rw_ref[:, own_q].astype(jnp.float32),
        precision=lax.Precision.HIGHEST,
        preferred_element_type=jnp.float32,
    )
    after_y(order[-1])
    result = home[0] + term
    for c in order[1:]:
        back_z(c).wait_recv()
        result = result + z_in[c].astype(jnp.float32)
    tgrad_ref[...] = result.astype(jnp.bfloat16)
    for copy in sent:
        copy.wait_send()


def write_out(*refs):
    count = len(refs) // 2
    copies = [
        pltpu.make_async_copy(refs[i], refs[count + i], refs[-1].at[i]) for i in range(count)
    ]
    for copy in reversed(copies):
        copy.start()
    for copy in copies:
        copy.wait()


def dense(tokens, out_grad, expert_ids, router_weight, w_gate, w_up, w_down):
    block, width = tokens.shape
    units = w_gate.shape[2]
    experts = router_weight.shape[1]
    n_ep, n_tp = lax.axis_size("ep"), lax.axis_size("tp")
    n_z = n_ep // 2
    feat = width // n_tp
    count = n_ep * block
    lanes = 128
    bf16, f32 = jnp.bfloat16, jnp.float32
    vmem = pl.BlockSpec(memory_space=pltpu.VMEM)
    hbm = pl.BlockSpec(memory_space=pltpu.HBM)
    dma = pltpu.SemaphoreType.DMA
    results = (
        ((block, feat), bf16),
        ((1, feat), f32),
        (w_gate.shape, bf16),
        (w_up.shape, bf16),
        (w_down.shape, bf16),
    )
    held = pl.pallas_call(
        dense_kernel,
        out_shape=tuple(pltpu.VMEM(shape, kind) for shape, kind in results),
        in_specs=[hbm, hbm, vmem, vmem, hbm, hbm, hbm],
        out_specs=(vmem,) * len(results),
        scratch_shapes=[
            pltpu.VMEM((2, count, width), bf16),
            pltpu.VMEM((width, units), bf16),
            pltpu.VMEM((width, units), bf16),
            pltpu.VMEM((units, width), bf16),
            pltpu.VMEM((n_ep, experts, lanes), f32),
            pltpu.VMEM((count, 2 * units), bf16),
            pltpu.VMEM((count, units), bf16),
            pltpu.VMEM((n_ep, lanes), f32),
            pltpu.VMEM((n_tp, n_ep, lanes), f32),
            pltpu.VMEM((experts, n_ep, lanes), f32),
            pltpu.VMEM((n_ep, experts, lanes), f32),
            pltpu.VMEM((n_z, 2, 2 * block, feat), f32),
            pltpu.VMEM((n_z, 2, 2 * block, feat), bf16),
            pltpu.VMEM((n_z, 2, 2 * block, feat), bf16),
            pltpu.VMEM((n_z, 2 * block, feat), bf16),
            pltpu.VMEM((n_z, 2 * block, feat), bf16),
            pltpu.VMEM((n_z, block, feat), bf16),
            pltpu.VMEM((n_z, block, feat), bf16),
            pltpu.VMEM((n_z, block, feat), bf16),
            pltpu.VMEM((n_z, block, feat), bf16),
            dma((5,)),
            dma((n_z,)), dma((n_z,)), dma((n_z,)), dma((n_z,)),
            dma((n_z, 2)), dma((n_z, 2)), dma((n_z, 2)), dma((n_z, 2)),
            dma((n_ep,)), dma((n_ep,)), dma((n_tp,)), dma((n_tp,)), dma((n_ep,)), dma((n_ep,)),
            dma((n_z,)), dma((n_z,)), dma((n_z,)), dma((n_z,)),
            dma((n_z,)), dma((n_z,)), dma((n_z,)), dma((n_z,)),
        ],
        compiler_params=pltpu.CompilerParams(
            collective_id=0, has_side_effects=True, vmem_limit_bytes=40 * 1024 * 1024
        ),
    )(
        *[pltpu.with_memory_space_constraint(part, pltpu.HBM) for part in (tokens, out_grad)],
        expert_ids.T,
        router_weight.T,
        *[pltpu.with_memory_space_constraint(part, pltpu.HBM) for part in (w_gate, w_up, w_down)],
    )
    outs = pl.pallas_call(
        write_out,
        out_shape=tuple(jax.ShapeDtypeStruct(shape, kind) for shape, kind in results),
        in_specs=[vmem] * len(results),
        out_specs=(hbm,) * len(results),
        scratch_shapes=[dma((len(results),))],
        compiler_params=pltpu.CompilerParams(vmem_limit_bytes=16 * 1024 * 1024),
    )(*[pltpu.with_memory_space_constraint(part, pltpu.VMEM) for part in held])
    token_grad, router_grad, w_gate_grad, w_up_grad, w_down_grad = outs
    return (token_grad, router_grad.T, w_gate_grad, w_up_grad, w_down_grad)


def per_device(tokens, out_grad, expert_ids, router_weight, w_gate, w_up, w_down):
    tok_dev, top_count = expert_ids.shape
    expert_count = router_weight.shape[1]
    tp_count = lax.axis_size("tp")
    capacity = min(
        tok_dev,
        tp_count * max(1, (2 * tok_dev * top_count // expert_count + tp_count - 1) // tp_count),
    )
    full = capacity == tok_dev and tp_count == 4 and lax.axis_size("ep") % 2 == 0
    return (dense if full else slotted)(
        tokens, out_grad, expert_ids, router_weight, w_gate, w_up, w_down
    )


def solution(mesh):
    in_specs = (
        P("ep", None),
        P("ep", None),
        P("ep", None),
        P(),
        P("ep", None, "tp"),
        P("ep", None, "tp"),
        P("ep", "tp", None),
    )
    out_specs = (
        P("ep", "tp"),
        P("tp", "ep"),
        P("ep", None, "tp"),
        P("ep", None, "tp"),
        P("ep", "tp", None),
    )
    return jax.shard_map(
        per_device, mesh=mesh, in_specs=in_specs, out_specs=out_specs, check_vma=False
    )
```

profile of v0, /device:TPU:0, one launch (start us, length us, event | category | flops | bytes accessed | tf_op | source)
XLA Modules:
  0.0 58.1 jit_solution(14093179156272259794)
XLA Ops:
  0.6 0.0 copy-start
  0.6 0.7 %copy-done = bf16[2048,8]{0,1:T(8,128)(2,1)S(1)} copy-done((bf16[2048,8]{0,1:T(8,128)(2,1)S(1)}, bf16[2048,8]{0,1:T(8,128)(2,1)}, u32[]{:S(2)}) %copy-start) | copy-done | bytes 32792
  1.4 0.0 copy-start.1
  1.4 0.7 %copy-done.1 = s32[48,4]{0,1:T(4,128)S(1)} copy-done((s32[48,4]{0,1:T(4,128)S(1)}, s32[48,4]{0,1:T(4,128)}, u32[]{:S(2)}) %copy-start.1) | copy-done | bytes 792
  2.1 53.7 %shard_map.110 = (bf16[48,512]{1,0:T(8,128)(2,1)S(1)}, f32[1,512]{1,0:T(1,128)S(1)}, bf16[1,2048,384]{2,1,0:T(8,128)(2,1)S(1)}, bf16[1,2048,384]{2,1,0:T(8,128)(2,1)S(1)}, bf16[1,384,2048]{2,1,0:T(8,128)(2,1)S(1)}) custom-call(bf16[48,2048]{1,0:T(8,128)(2,1)} %tok_ref.1, bf16[48,2048]{1,0:T(8,128)(2,1)} %og_ref.1, s32[4,48]{1,0:T(4,128)S(1)} %bitcast.4, ...), custom_call_target="tpu_custom_call" | custom-call | tf_op jit(solution)/shard_map/pallas_call | solution.py:490
  55.8 2.2 %shard_map.111 = (bf16[48,512]{1,0:T(8,128)(2,1)}, f32[1,512]{1,0:T(1,128)}, bf16[1,2048,384]{2,1,0:T(8,128)(2,1)}, bf16[1,2048,384]{2,1,0:T(8,128)(2,1)}, bf16[1,384,2048]{2,1,0:T(8,128)(2,1)}) custom-call(bf16[48,512]{1,0:T(8,128)(2,1)S(1)} %get-tuple-element.15.refs_0_, f32[1,512]{1,0:T(1,128)S(1)} %get-tuple-element.16.refs_1_, ...), custom_call_target="tpu_custom_call" | custom-call | tf_op jit(solution)/shard_map/pallas_call | solution.py:532
Async XLA Ops:
  0.6 0.8 %copy-start = (bf16[2048,8]{0,1:T(8,128)(2,1)S(1)}, bf16[2048,8]{0,1:T(8,128)(2,1)}, u32[]{:S(2)}) copy-start(bf16[2048,8]{0,1:T(8,128)(2,1)} %param.10) | copy-start | bytes 98308
  1.4 0.7 %copy-start.1 = (s32[48,4]{0,1:T(4,128)S(1)}, s32[48,4]{0,1:T(4,128)}, u32[]{:S(2)}) copy-start(s32[48,4]{0,1:T(4,128)} %param.9) | copy-start | bytes 2308
where the time goes:
time: 58.3 us; the launch traced here: 58.1 us
  Pallas kernels  56 us (96%)
  local copies, waits for them, and re-layouts  1.43 us (2%)
  between operations  0.65 us (1%)
    pallas_call x1, Pallas kernels, dense(): pl.pallas_call(dense_kernel, out_shape=tuple((pltpu.VMEM(shape, kind) for...  53.7 us
    pallas_call x1, Pallas kernels, dense(): pl.pallas_call(write_out, out_shape=tuple((jax.ShapeDtypeStruct(shape, ki...  2.23 us
    unnamed x4, local copies, waits for them, and re-layouts  1.43 us

commit v1 on v0

--- a/solution.py
+++ b/solution.py
@@ -135,20 +135,27 @@
     return (token_grad, router_grad, w_gate_grad, w_up_grad, w_down_grad)
 
 
+SCHEDULE = (
+    ("z", 1), ("p", 0), ("z", 2), ("r",), ("m", 0), ("f", 0), ("p", 1), ("z", 3), ("q", 0),
+    ("m", 1), ("f", 1), ("p", 2), ("am", 0), ("q", 1), ("m", 2), ("f", 2), ("p", 3), ("am", 1),
+    ("q", 2), ("ap", 0), ("m", 3), ("f", 3), ("ts",), ("q", 3), ("am", 2), ("ap", 1), ("w", 2),
+    ("am", 3), ("te",), ("w", 2), ("ap", 2), ("w", 4), ("ap", 3),
+)
+
+
 def dense_kernel(
-    tok_ref, og_ref, ids_ref, rw_ref, wg_ref, wu_ref, wd_ref,
+    tok_ref, og_ref, ids_hbm, rw_hbm, wg_ref, wu_ref, wd_ref,
     tgrad_ref, rgrad_ref, wgg, wug, wdg,
-    rows_v, wg, wu, wd, gates, dpre, weighted, part_scores, tp_scores, scores, dlog,
-    own_part, mate_out, mate_in, x_out, x_in, y_out, y_in, z_out, z_in,
-    load_sem, z_s, z_r, y_s, y_r, x_s, x_r, m_s, m_r,
-    g_s, g_r, t_s, t_r, s_s, s_r, rm_s, rm_r, rx_s, rx_r, ry_s, ry_r, rz_s, rz_r,
+    ids_ref, rw_ref, rows_v, wg, wu, wd, gates, dpre, weighted, part_scores, tp_scores, scores, dlog,
+    own_part, mate_out, mate_in, p_out, p_in, z_out, z_in,
+    load_sem, z_s, z_r, p_s, p_r, m_s, m_r,
+    g_s, g_r, t_s, t_r, s_s, s_r, rm_s, rm_r, rp_s, rp_r, rz_s, rz_r,
 ):
     block, width = tok_ref.shape
     units = wd.shape[0]
     n_ep, experts, lanes = gates.shape
     n_tp = lax.axis_size("tp")
     n_z = n_ep // 2
-    pair = 2 * block
     feat = width // n_tp
     ep = lax.axis_index("ep")
     tp = lax.axis_index("tp")
@@ -156,10 +163,13 @@
     x, core = tp // 2, tp % 2
     y_dev = (z * 2 + 1 - y, tp)
     x_dev = (ep, (1 - x) * 2 + core)
+    d_dev = (z * 2 + 1 - y, (1 - x) * 2 + core)
     m_dev = (ep, x * 2 + 1 - core)
-
-    def z_dev(hop):
-        return (((z + hop) % n_z) * 2 + y, tp)
+    plane = (y_dev, x_dev, d_dev)
+    near = (z, 1 + z % 2, (2 + 3 * z) % 5, 3 * (1 - z // 2))
+
+    def z_dev(i):
+        return (near[i] * 2 + y, tp)
 
     def ep_dev(hop):
         return ((ep + hop) % n_ep, tp)
@@ -183,14 +193,16 @@
     loads = [
         pltpu.make_async_copy(tok_ref, rows_v.at[0, mine, :], load_sem.at[0]),
         pltpu.make_async_copy(og_ref, rows_v.at[1, mine, :], load_sem.at[1]),
-        pltpu.make_async_copy(wg_ref.at[0], wg, load_sem.at[2]),
-        pltpu.make_async_copy(wu_ref.at[0], wu, load_sem.at[3]),
-        pltpu.make_async_copy(wd_ref.at[0], wd, load_sem.at[4]),
+        pltpu.make_async_copy(ids_hbm, ids_ref, load_sem.at[2]),
+        pltpu.make_async_copy(rw_hbm, rw_ref, load_sem.at[3]),
+        pltpu.make_async_copy(wg_ref.at[0], wg, load_sem.at[4]),
+        pltpu.make_async_copy(wu_ref.at[0], wu, load_sem.at[5]),
+        pltpu.make_async_copy(wd_ref.at[0], wd, load_sem.at[6]),
     ]
     for load in loads:
         load.start()
     barrier = pltpu.get_barrier_semaphore()
-    partners = [ep_dev(k) for k in range(1, n_ep)] + [tp_dev(k) for k in range(1, n_tp)]
+    partners = [ep_dev(k) for k in range(1, n_ep)] + [tp_dev(k) for k in range(1, n_tp)] + [d_dev]
     for dev in partners:
         pl.semaphore_signal(barrier, inc=1, device_id=dev, device_id_type=MESH)
     pl.semaphore_wait(barrier, len(partners))
@@ -200,35 +212,41 @@
         copy.start()
         sent.append(copy)
 
+    own_q, other_q = cols(tp), cols((1 - x) * 2 + core)
+    mate_q = (cols(x * 2 + 1 - core), cols((1 - x) * 2 + 1 - core))
+
+    def piece(first, count, quarter):
+        return rows_v.at[:, rows(first, count), quarter]
+
+    def z_send(i):
+        p = piece(ep, 1, own_q)
+        return remote(p, p, z_s.at[i], z_r.at[z], z_dev(i))
+
+    def z_recv(i):
+        p = piece(near[i] * 2 + y, 1, own_q)
+        return remote(p, p, z_s.at[i], z_r.at[near[i]], z_dev(i))
+
+    def p_copy(i, kind, first, quarter=None):
+        p = piece(first, 1, own_q if quarter is None else quarter)
+        return remote(p, p, p_s.at[i, kind], p_r.at[i, kind], plane[min(kind, 2)])
+
+    def m_copy(i, which, first, count, quarter):
+        p = piece(first, count, quarter)
+        return remote(p, p, m_s.at[i, which], m_r.at[i, which], m_dev)
+
+    def y_home(which, first, quarter):
+        p = piece(first, 1, quarter)
+        return remote(p, p, p_s.at[0, which], p_r.at[0, which], y_dev)
+
     loads[0].wait()
     loads[1].wait()
-    own_q, other_q = cols(tp), cols((1 - x) * 2 + core)
-
-    def piece(first, count, quarter):
-        return rows_v.at[:, rows(first, count), quarter]
-
-    def z_copy(hop, first):
-        p = piece(first, 1, own_q)
-        return remote(p, p, z_s.at[hop], z_r.at[hop], z_dev(hop))
-
-    def y_copy(c, first):
-        p = piece(first, 1, own_q)
-        return remote(p, p, y_s.at[c], y_r.at[c], y_dev)
-
-    def x_copy(c, which, first, quarter=None):
-        p = piece(first, 1, own_q if quarter is None else quarter)
-        return remote(p, p, x_s.at[c, which], x_r.at[c, which], x_dev)
-
-    def m_copy(c, which, first, count, quarter):
-        p = piece(first, count, quarter)
-        return remote(p, p, m_s.at[c, which], m_r.at[c, which], m_dev)
-
-    mate_q = (cols(x * 2 + 1 - core), cols((1 - x) * 2 + 1 - core))
-    launch(y_copy(0, ep))
-    order = [0] + sorted(range(1, n_z), key=lambda c: min(c, n_z - c))
-    for c in order[1:]:
-        launch(z_copy(c, ep))
-
+    launch(y_home(0, ep, own_q))
+    for i in range(1, n_z):
+        launch(z_send(i))
+    launch(y_home(1, ep, other_q))
+
+    loads[2].wait()
+    loads[3].wait()
     logits = contract_last(rw_ref[...], rows_v[0, mine, :])
     expert = lax.broadcasted_iota(jnp.int32, (experts, block), 0)
     hot = jnp.zeros((experts, block), jnp.float32)
@@ -246,124 +264,41 @@
     for hop in range(1, n_ep):
         launch(gate_copy(hop, ep))
 
-    for c in order:
-        zs = (z + n_z - c) % n_z
-        a, b = zs * 2 + y, zs * 2 + 1 - y
-        if c > 0:
-            z_copy(c, a).wait_recv()
-            launch(y_copy(c, a))
-            launch(x_copy(c, 0, a))
-        y_copy(c, b).wait_recv()
-        launch(x_copy(c, 1, b))
-        if c > 0:
-            launch(m_copy(c, 0, zs * 2, 2, own_q))
+    def pair(i):
+        return near[i] * 2 + y, near[i] * 2 + 1 - y
+
+    def z_event(i):
+        a, _ = pair(i)
+        z_recv(i).wait_recv()
+        for kind in range(3):
+            launch(p_copy(i, kind, a))
+        launch(m_copy(i, 0, a, 1, own_q))
+
+    def plane_event(i):
+        a, b = pair(i)
+        if i == 0:
+            y_home(0, b, own_q).wait_recv()
+            launch(m_copy(0, 1, b, 1, own_q))
+            y_home(1, b, other_q).wait_recv()
+            launch(m_copy(0, 2, b, 1, other_q))
         else:
-            launch(m_copy(c, 0, b, 1, own_q))
-    for hop in range(1, n_ep):
-        gate_copy(hop, (ep + n_ep - hop) % n_ep).wait_recv()
-    for load in loads[2:]:
-        load.wait()
-
-    def tp_score_copy(hop):
-        return remote(part_scores, tp_scores.at[hop], t_s.at[hop], t_r.at[hop], tp_dev(hop))
-
-    def score_copy(hop, src):
-        return remote(scores.at[src], scores.at[src], s_s.at[hop], s_r.at[hop], ep_dev(hop))
-
-    def back_mate(c):
-        return remote(mate_out.at[c], mate_in.at[c], rm_s.at[c], rm_r.at[c], m_dev)
-
-    def crossed(c):
-        return order.index(c) % 2 == 1
-
-    def back_x(c):
-        return remote(x_out.at[c], x_in.at[c], rx_s.at[c], rx_r.at[c], y_dev if crossed(c) else x_dev)
-
-    def back_y(c):
-        return remote(y_out.at[c], y_in.at[c], ry_s.at[c], ry_r.at[c], x_dev if crossed(c) else y_dev)
-
-    def back_z(c):
-        return remote(z_out.at[c], z_in.at[c], rz_s.at[c], rz_r.at[c], z_dev(n_z - c))
-
-    def produce(c):
-        here = rows((z + n_z - c) % n_z * 2, 2)
-        dg = dpre[here, 0:units]
-        du = dpre[here, units : 2 * units]
-        for half in range(2):
-            for side in range(2):
-                q = half * 2 + (1 - core if side == 0 else core)
-                span = cols(q)
-                value = contract_last(dg, wg[span, :]) + contract_last(du, wu[span, :])
-                if side == 0:
-                    mate_out[c, half] = value.astype(jnp.bfloat16)
-                else:
-                    own_part[c, half] = value
-        launch(back_mate(c))
-
-    def after_mate(c):
-        back_mate(c).wait_recv()
-        if crossed(c):
-            theirs = rows(1 - y, 1)
-            for half in range(2):
-                x_out[c, half * block : (half + 1) * block] = (
-                    own_part[c, half, theirs, :] + mate_in[c, half, theirs, :].astype(jnp.float32)
-                ).astype(jnp.bfloat16)
+            p_copy(i, 0, b).wait_recv()
+            launch(m_copy(i, 1, b, 1, own_q))
+            p_copy(i, 1, a, other_q).wait_recv()
+            p_copy(i, 2, b, other_q).wait_recv()
+            launch(m_copy(i, 2, near[i] * 2, 2, other_q))
+
+    def mate_event(i):
+        a, b = pair(i)
+        m_copy(i, 1, b, 1, mate_q[0]).wait_recv()
+        if i == 0:
+            m_copy(i, 2, b, 1, mate_q[1]).wait_recv()
         else:
-            x_out[c] = (own_part[c, 1 - x] + mate_in[c, 1 - x].astype(jnp.float32)).astype(jnp.bfloat16)
-        launch(back_x(c))
-
-    def after_x(c):
-        back_x(c).wait_recv()
-        if crossed(c):
-            for half in range(2):
-                own_part[c, half, rows(y, 1), :] = (
-                    own_part[c, half, rows(y, 1), :]
-                    + mate_in[c, half, rows(y, 1), :].astype(jnp.float32)
-                    + x_in[c, half * block : (half + 1) * block].astype(jnp.float32)
-                )
-            y_out[c] = own_part[c, 1 - x, rows(y, 1), :].astype(jnp.bfloat16)
-        else:
-            total = own_part[c, x] + mate_in[c, x].astype(jnp.float32) + x_in[c].astype(jnp.float32)
-            own_part[c, x] = total
-            y_out[c] = own_part[c, x, rows(1 - y, 1), :].astype(jnp.bfloat16)
-        launch(back_y(c))
-
-    home = {}
-
-    def after_y(c):
-        back_y(c).wait_recv()
-        total = own_part[c, x, rows(y, 1), :] + y_in[c].astype(jnp.float32)
-        if c > 0:
-            z_out[c] = total.astype(jnp.bfloat16)
-            launch(back_z(c))
-        else:
-            home[0] = total
-
-    tiles = 8
-    tile = width // tiles
-
-    def in_grad(i):
-        span = pl.ds(i * tile, tile)
-        value = contract_first(rows_v[0, :, span], dpre[...]).astype(jnp.bfloat16)
-        wgg[0, span, :] = value[:, 0:units]
-        wug[0, span, :] = value[:, units : 2 * units]
-
-    def down_grad(i):
-        span = pl.ds(i * feat, feat)
-        wdg[0, :, span] = contract_first(weighted[...], rows_v[1, :, span]).astype(jnp.bfloat16)
-
-    for c in order:
-        zs = (z + n_z - c) % n_z
-        a, b = zs * 2 + y, zs * 2 + 1 - y
-        first, count = (zs * 2, 2) if c > 0 else (b, 1)
-        if c > 0:
-            x_copy(c, 0, a, other_q).wait_recv()
-        x_copy(c, 1, b, other_q).wait_recv()
-        launch(m_copy(c, 1, first, count, other_q))
-        if c != order[0]:
-            produce(previous)
-        m_copy(c, 0, first, count, mate_q[0]).wait_recv()
-        m_copy(c, 1, first, count, mate_q[1]).wait_recv()
+            m_copy(i, 0, a, 1, mate_q[0]).wait_recv()
+            m_copy(i, 2, near[i] * 2, 2, mate_q[1]).wait_recv()
+
+    def forward(i):
+        zs = near[i]
         here = rows(zs * 2, 2)
         in_rows = rows_v[0, here, :]
         grad_rows = rows_v[1, here, :]
@@ -372,31 +307,96 @@
         back = contract_last(grad_rows, wd[...])
         hidden, slope, up_slope = activation_parts(gate_pre, up_pre)
         columns = []
-        for i in range(2):
-            row = gates[zs * 2 + i, pl.ds(ep, 1), :]
+        for k in range(2):
+            row = gates[zs * 2 + k, pl.ds(ep, 1), :]
             columns.append(jnp.broadcast_to(row, (lanes, lanes)).T[:block])
         weight = jnp.concatenate(columns, axis=0)
         weight = jnp.concatenate([weight] * (units // lanes), axis=1)
         product = hidden * back
         folded = product[:, 0:lanes]
-        for i in range(1, units // lanes):
-            folded = folded + product[:, i * lanes : (i + 1) * lanes]
-        for i in range(2):
+        for k in range(1, units // lanes):
+            folded = folded + product[:, k * lanes : (k + 1) * lanes]
+        for k in range(2):
             tall = jnp.concatenate(
-                [folded[i * block : (i + 1) * block], jnp.zeros((lanes - block, lanes), jnp.float32)],
+                [folded[k * block : (k + 1) * block], jnp.zeros((lanes - block, lanes), jnp.float32)],
                 axis=0,
             )
-            part_scores[pl.ds(zs * 2 + i, 1), :] = jnp.sum(tall.T, axis=0, keepdims=True)
+            part_scores[pl.ds(zs * 2 + k, 1), :] = jnp.sum(tall.T, axis=0, keepdims=True)
         d_hidden = weight * back
         dpre[here, 0:units] = (d_hidden * slope).astype(jnp.bfloat16)
         dpre[here, units : 2 * units] = (d_hidden * up_slope).astype(jnp.bfloat16)
         weighted[here, :] = (weight * hidden).astype(jnp.bfloat16)
-        if c != order[0]:
-            after_mate(previous)
-        previous = c
-
-    for hop in range(1, n_tp):
-        launch(tp_score_copy(hop))
+
+    def tp_score_copy(hop):
+        return remote(part_scores, tp_scores.at[hop], t_s.at[hop], t_r.at[hop], tp_dev(hop))
+
+    def score_copy(hop, src):
+        return remote(scores.at[src], scores.at[src], s_s.at[hop], s_r.at[hop], ep_dev(hop))
+
+    def back_mate(i):
+        return remote(mate_out.at[i], mate_in.at[i], rm_s.at[i], rm_r.at[i], m_dev)
+
+    def back_plane(i, kind):
+        return remote(p_out.at[i, kind], p_in.at[i, kind], rp_s.at[i, kind], rp_r.at[i, kind], plane[kind])
+
+    def back_send(i):
+        return remote(z_out.at[i], z_in.at[z], rz_s.at[i], rz_r.at[z], z_dev(i))
+
+    def back_recv(i):
+        return remote(z_out.at[i], z_in.at[near[i]], rz_s.at[i], rz_r.at[near[i]], z_dev(i))
+
+    def produce(i):
+        here = rows(near[i] * 2, 2)
+        dg = dpre[here, 0:units]
+        du = dpre[here, units : 2 * units]
+        for side in range(2):
+            for half in range(2):
+                q = half * 2 + (1 - core if side == 0 else core)
+                span = cols(q)
+                value = contract_last(dg, wg[span, :]) + contract_last(du, wu[span, :])
+                if side == 0:
+                    mate_out[i, half] = value.astype(jnp.bfloat16)
+                else:
+                    own_part[i, half] = value
+            if side == 0:
+                launch(back_mate(i))
+
+    def after_mate(i):
+        back_mate(i).wait_recv()
+        ours, theirs = rows(y, 1), rows(1 - y, 1)
+        for kind, (half, part) in enumerate(((x, theirs), (1 - x, ours), (1 - x, theirs))):
+            p_out[i, kind] = (
+                own_part[i, half, part, :] + mate_in[i, half, part, :].astype(jnp.float32)
+            ).astype(jnp.bfloat16)
+            launch(back_plane(i, kind))
+
+    home = {}
+
+    def after_plane(i):
+        ours = rows(y, 1)
+        total = own_part[i, x, ours, :] + mate_in[i, x, ours, :].astype(jnp.float32)
+        for kind in range(3):
+            back_plane(i, kind).wait_recv()
+            total = total + p_in[i, kind].astype(jnp.float32)
+        if i > 0:
+            z_out[i] = total.astype(jnp.bfloat16)
+            launch(back_send(i))
+        else:
+            own_part[0, x, ours, :] = total
+
+    tiles = 8
+    tile = width // tiles
+
+    def in_grad(i):
+        span = pl.ds(i * tile, tile)
+        value = contract_first(rows_v[0, :, span], dpre[...]).astype(jnp.bfloat16)
+        wgg[0, span, :] = value[:, 0:units]
+        wug[0, span, :] = value[:, units : 2 * units]
+
+    def down_grad(i):
+        span = pl.ds(i * feat, feat)
+        wdg[0, :, span] = contract_first(weighted[...], rows_v[1, :, span]).astype(jnp.bfloat16)
+
     pieces = [functools.partial(in_grad, i) for i in range(tiles)]
     pieces += [functools.partial(down_grad, i) for i in range(n_tp)]
 
@@ -405,23 +405,31 @@
             piece()
         del pieces[:amount]
 
-    produce(order[-1])
-    work(2)
-    after_mate(order[-1])
-    total = part_scores[...]
-    for hop in range(1, n_tp):
-        tp_score_copy(hop).wait_recv()
-        total = total + tp_scores[hop]
-    scores[ep] = total
-    for hop in range(1, n_ep):
-        launch(score_copy(hop, ep))
-    work(2)
-    for i, c in enumerate(order):
-        after_x(c)
-        if i > 0:
-            after_y(order[i - 1])
-        if i < n_z - 1:
-            work(3)
+    def ready():
+        for hop in range(1, n_ep):
+            gate_copy(hop, (ep + n_ep - hop) % n_ep).wait_recv()
+        for load in loads[4:]:
+            load.wait()
+
+    def tp_send():
+        for hop in range(1, n_tp):
+            launch(tp_score_copy(hop))
+
+    def tp_event():
+        total = part_scores[...]
+        for hop in range(1, n_tp):
+            tp_score_copy(hop).wait_recv()
+            total = total + tp_scores[hop]
+        scores[ep] = total
+        for hop in range(1, n_ep):
+            launch(score_copy(hop, ep))
+
+    steps = {
+        "z": z_event, "p": plane_event, "m": mate_event, "f": forward, "q": produce,
+        "am": after_mate, "ap": after_plane, "w": work,
+    }
+    for name, *args in SCHEDULE:
+        {**steps, "r": ready, "ts": tp_send, "te": tp_event}[name](*args)
     work(len(pieces))
     for hop in range(1, n_ep):
         score_copy(hop, (ep + n_ep - hop) % n_ep).wait_recv()
@@ -446,11 +454,10 @@
         precision=lax.Precision.HIGHEST,
         preferred_element_type=jnp.float32,
     )
-    after_y(order[-1])
-    result = home[0] + term
-    for c in order[1:]:
-        back_z(c).wait_recv()
-        result = result + z_in[c].astype(jnp.float32)
+    result = own_part[0, x, rows(y, 1), :] + term
+    for i in range(1, n_z):
+        back_recv(i).wait_recv()
+        result = result + z_in[near[i]].astype(jnp.float32)
     tgrad_ref[...] = result.astype(jnp.bfloat16)
     for copy in sent:
         copy.wait_send()
@@ -470,6 +477,7 @@
 def dense(tokens, out_grad, expert_ids, router_weight, w_gate, w_up, w_down):
     block, width = tokens.shape
     units = w_gate.shape[2]
+    top_count = expert_ids.shape[1]
     experts = router_weight.shape[1]
     n_ep, n_tp = lax.axis_size("ep"), lax.axis_size("tp")
     n_z = n_ep // 2
@@ -490,9 +498,11 @@
     held = pl.pallas_call(
         dense_kernel,
         out_shape=tuple(pltpu.VMEM(shape, kind) for shape, kind in results),
-        in_specs=[hbm, hbm, vmem, vmem, hbm, hbm, hbm],
+        in_specs=[hbm] * 7,
         out_specs=(vmem,) * len(results),
         scratch_shapes=[
+            pltpu.VMEM((top_count, block), jnp.int32),
+            pltpu.VMEM((experts, width), bf16),
             pltpu.VMEM((2, count, width), bf16),
             pltpu.VMEM((width, units), bf16),
             pltpu.VMEM((width, units), bf16),
@@ -507,27 +517,23 @@
             pltpu.VMEM((n_z, 2, 2 * block, feat), f32),
             pltpu.VMEM((n_z, 2, 2 * block, feat), bf16),
             pltpu.VMEM((n_z, 2, 2 * block, feat), bf16),
-            pltpu.VMEM((n_z, 2 * block, feat), bf16),
-            pltpu.VMEM((n_z, 2 * block, feat), bf16),
+            pltpu.VMEM((n_z, 3, block, feat), bf16),
+            pltpu.VMEM((n_z, 3, block, feat), bf16),
             pltpu.VMEM((n_z, block, feat), bf16),
             pltpu.VMEM((n_z, block, feat), bf16),
-            pltpu.VMEM((n_z, block, feat), bf16),
-            pltpu.VMEM((n_z, block, feat), bf16),
-            dma((5,)),
-            dma((n_z,)), dma((n_z,)), dma((n_z,)), dma((n_z,)),
-            dma((n_z, 2)), dma((n_z, 2)), dma((n_z, 2)), dma((n_z, 2)),
+            dma((7,)),
+            dma((n_z,)), dma((n_z,)), dma((n_z, 3)), dma((n_z, 3)), dma((n_z, 3)), dma((n_z, 3)),
             dma((n_ep,)), dma((n_ep,)), dma((n_tp,)), dma((n_tp,)), dma((n_ep,)), dma((n_ep,)),
-            dma((n_z,)), dma((n_z,)), dma((n_z,)), dma((n_z,)),
-            dma((n_z,)), dma((n_z,)), dma((n_z,)), dma((n_z,)),
+            dma((n_z,)), dma((n_z,)), dma((n_z, 3)), dma((n_z, 3)), dma((n_z,)), dma((n_z,)),
         ],
         compiler_params=pltpu.CompilerParams(
             collective_id=0, has_side_effects=True, vmem_limit_bytes=40 * 1024 * 1024
         ),
     )(
-        *[pltpu.with_memory_space_constraint(part, pltpu.HBM) for part in (tokens, out_grad)],
-        expert_ids.T,
-        router_weight.T,
-        *[pltpu.with_memory_space_constraint(part, pltpu.HBM) for part in (w_gate, w_up, w_down)],
+        *[
+            pltpu.with_memory_space_constraint(part, pltpu.HBM)
+            for part in (tokens, out_grad, expert_ids.T, router_weight.T, w_gate, w_up, w_down)
+        ],
     )
     outs = pl.pallas_call(
         write_out,
@@ -549,7 +555,7 @@
         tok_dev,
         tp_count * max(1, (2 * tok_dev * top_count // expert_count + tp_count - 1) // tp_count),
     )
-    full = capacity == tok_dev and tp_count == 4 and lax.axis_size("ep") % 2 == 0
+    full = capacity == tok_dev and tp_count == 4 and lax.axis_size("ep") == 8
     return (dense if full else slotted)(
         tokens, out_grad, expert_ids, router_weight, w_gate, w_up, w_down
     )

time: 58.3 us -> 46.8 us (0.80)
  Pallas kernels: 56 us -> 46 us
  local copies, waits for them, and re-layouts: 1.43 us -> 0 us
    pallas_call x1, Pallas kernels: 53.7 us -> 43.8 us  [dense(): pl.pallas_call(dense_kernel, out_shape=tuple((pltpu.VMEM(shape, kind) for...]
    unnamed x4 -> x0, local copies, waits for them, and re-layouts: 1.43 us -> none
where the time goes in v1:
time: 46.8 us; the launch traced here: 46.7 us
  Pallas kernels  46 us (98%)
  between operations  0.64 us (1%)
    pallas_call x1, Pallas kernels, dense(): pl.pallas_call(dense_kernel, out_shape=tuple((pltpu.VMEM(shape, kind) for...  43.8 us
    pallas_call x1, Pallas kernels, dense(): pl.pallas_call(write_out, out_shape=tuple((jax.ShapeDtypeStruct(shape, ki...  2.23 us

profile of v1, /device:TPU:0, one launch (start us, length us, event | category | flops | bytes accessed | tf_op | source)
XLA Modules:
  0.0 46.7 jit_solution(14601393463735111663)
XLA Ops:
  0.6 43.8 %shard_map.110 = (bf16[48,512]{1,0:T(8,128)(2,1)S(1)}, f32[1,512]{1,0:T(1,128)S(1)}, bf16[1,2048,384]{2,1,0:T(8,128)(2,1)S(1)}, bf16[1,2048,384]{2,1,0:T(8,128)(2,1)S(1)}, bf16[1,384,2048]{2,1,0:T(8,128)(2,1)S(1)}) custom-call(bf16[48,2048]{1,0:T(8,128)(2,1)} %tok_ref.1, bf16[48,2048]{1,0:T(8,128)(2,1)} %og_ref.1, s32[4,48]{1,0:T(4,128)} %bitcast.4, ...), custom_call_target="tpu_custom_call" | custom-call | tf_op jit(solution)/shard_map/pallas_call | solution.py:498
  44.4 2.2 %shard_map.111 = (bf16[48,512]{1,0:T(8,128)(2,1)}, f32[1,512]{1,0:T(1,128)}, bf16[1,2048,384]{2,1,0:T(8,128)(2,1)}, bf16[1,2048,384]{2,1,0:T(8,128)(2,1)}, bf16[1,384,2048]{2,1,0:T(8,128)(2,1)}) custom-call(bf16[48,512]{1,0:T(8,128)(2,1)S(1)} %get-tuple-element.15.refs_0_, f32[1,512]{1,0:T(1,128)S(1)} %get-tuple-element.16.refs_1_, ...), custom_call_target="tpu_custom_call" | custom-call | tf_op jit(solution)/shard_map/pallas_call | solution.py:538
